TPU v7x, 32 devices: a whole 2x2x4 slice. The times are simulated.
32 devices in a mesh: grp: 2 (over y), ep: 4 (over z), tp: 4 (over x, core).
Axes of the slice: x: 2, y: 2, z: 4, core: 2. Of those that a mesh axis runs over, the one named last changes fastest.
Arguments:
- conv_x: bfloat16 [8192, 2048], P(('grp', 'ep', 'tp')), parts along dimension 0, may hold values from -6 to 6
- conv_c: bfloat16 [8192, 2048], P(('grp', 'ep', 'tp')), parts along dimension 0, may hold values from -6 to 6
- conv_b: bfloat16 [8192, 2048], P(('grp', 'ep', 'tp')), parts along dimension 0, may hold values from -6 to 6
- conv_taps: float32 [3, 2048], replicated, may hold values from -3.5 to 3.5
- w_out: bfloat16 [2048, 2048], P('tp'), may hold values from -0.125 to 0.125
- tokens_b: bfloat16 [4096, 2048], P(('grp', 'ep', 'tp')), parts along dimension 0, may hold values from -6 to 6
- norm_gain: float32 [2048], replicated, may hold values from 0.1 to 1.9
- route_b: int32 [4096, 2], P(('grp', 'ep', 'tp')), parts along dimension 0, may hold values from 0 to 3, all different within a row; in each aligned block of 128 rows (0 to 127, 128 to 255, ...) at most 128 rows name the same one
- route_weights: float32 [4096, 2], P(('grp', 'ep', 'tp')), parts along dimension 0, may hold values from 0.1 to 1
- w_gate: bfloat16 [4, 2048, 1024], P('ep', None, 'tp'), may hold values from -0.125 to 0.125
- w_up: bfloat16 [4, 2048, 1024], P('ep', None, 'tp'), may hold values from -0.125 to 0.125
- w_down: bfloat16 [4, 1024, 2048], P('ep', 'tp'), may hold values from -0.1875 to 0.1875
Outputs:
- mixed_a: bfloat16 [8192, 2048], P(('grp', 'ep', 'tp')), parts along dimension 0
- experts_b: bfloat16 [4096, 2048], P(('grp', 'ep', 'tp')), parts along dimension 0
There are 2 independent parts, one for each index of `grp`. A program takes and returns all parts, laid end to end along the dimension named above; an argument that names none is the same for every part. Nothing has to cross between parts.
Inputs may be any that keep to these rules, and one draw needn't show every extreme that they name: `route_b`: the 2 experts of a row differ. Within the 128 rows of one device no expert is named more than 128 times, and in every draw some device names some expert exactly 128 times.
All inputs are finite; a program needn't handle non-finite values.
Results may differ from a plain program's by a relative error of at most 0.012.
Values may be sent and summed in bfloat16 or wider, within the bound.
A program may use at most 128 MiB of HBM per device.

v0:
```python
import jax
import jax.numpy as jnp
from jax import lax
from jax.sharding import PartitionSpec as P

D = 2048
TOPK = 2


def shifted(x, axis, by):
    size = lax.axis_size(axis)
    pairs = [(i, i + by) for i in range(size) if 0 <= i + by < size]
    return lax.ppermute(x, axis, pairs)


def slot_targets(route, experts, capacity):
    flat = route.reshape(-1)
    onehot = (flat[:, None] == jnp.arange(experts, dtype=jnp.int32)[None, :]).astype(jnp.int32)
    earlier = jnp.cumsum(onehot, axis=0) - onehot
    ranks = jnp.sum(earlier * onehot, axis=1).reshape(route.shape)
    return route * capacity + ranks


def fill_slots(targets, slot_total, filler):
    token_ids = jnp.repeat(jnp.arange(filler, dtype=jnp.int32), targets.shape[1])
    return jnp.full((slot_total,), filler, jnp.int32).at[targets.reshape(-1)].set(token_ids)


def expert_hidden(rows, weight_gate, weight_up):
    gate_val = jnp.dot(rows, weight_gate, preferred_element_type=jnp.float32)
    up_val = jnp.dot(rows, weight_up, preferred_element_type=jnp.float32)
    return (jax.nn.silu(gate_val) * up_val).astype(jnp.bfloat16)


def per_device(
    conv_x,
    conv_c,
    conv_b,
    conv_taps,
    w_out,
    tokens_b,
    norm_gain,
    route_b,
    route_weights,
    w_gate,
    w_up,
    w_down,
):
    rows_mix = conv_x.shape[0]
    reach_rows = conv_taps.shape[0] - 1
    mixed_u = (conv_c.astype(jnp.float32) * conv_x.astype(jnp.float32)).astype(jnp.bfloat16)
    before = shifted(mixed_u[rows_mix - reach_rows :], ("ep", "tp"), 1)
    extended = jnp.concatenate([before, mixed_u], axis=0)
    filtered = jnp.zeros(mixed_u.shape, jnp.float32)
    for shift_tap in range(reach_rows + 1):
        filtered = filtered + conv_taps[shift_tap][None, :] * extended[
            shift_tap : shift_tap + rows_mix
        ].astype(jnp.float32)
    gated_rows = (conv_b.astype(jnp.float32) * filtered).astype(jnp.bfloat16)
    mixed_out = jnp.dot(
        gated_rows,
        lax.all_gather(w_out, "tp", axis=0, tiled=True),
        preferred_element_type=jnp.float32,
    )
    mixed_a = mixed_out.astype(jnp.bfloat16)
    tokens_f = tokens_b.astype(jnp.float32)
    normed = (
        tokens_f
        * lax.rsqrt(jnp.mean(tokens_f * tokens_f, axis=-1, keepdims=True) + 1e-06)
        * norm_gain
    ).astype(jnp.bfloat16)
    experts = lax.axis_size("ep")
    rows_exp = route_b.shape[0]
    capacity = 2 * rows_exp * TOPK // experts
    slot_total = experts * capacity
    targets = slot_targets(route_b, experts, capacity)
    weight_gate = w_gate[0]
    weight_up = w_up[0]
    weight_down = w_down[0]
    padded_rows = jnp.concatenate([normed, jnp.zeros((1, D), jnp.bfloat16)], axis=0)
    outgoing = padded_rows[fill_slots(targets, slot_total, rows_exp)]
    arrived = lax.all_to_all(outgoing, "ep", split_axis=0, concat_axis=0, tiled=True)
    hidden = expert_hidden(
        lax.all_gather(arrived, "tp", axis=0, tiled=True), weight_gate, weight_up
    )
    summed = lax.psum_scatter(
        jnp.dot(hidden, weight_down, preferred_element_type=jnp.float32).astype(jnp.bfloat16),
        "tp",
        scatter_dimension=0,
        tiled=True,
    )
    returned = lax.all_to_all(summed, "ep", split_axis=0, concat_axis=0, tiled=True)
    picked = returned[targets]
    shares = route_weights / jnp.sum(route_weights, axis=-1, keepdims=True)
    experts_b = jnp.sum(picked.astype(jnp.float32) * shares[:, :, None], axis=1).astype(
        jnp.bfloat16
    )
    return (mixed_a, experts_b)


def solution(mesh):
    return jax.shard_map(
        per_device,
        mesh=mesh,
        in_specs=(
            P(("grp", "ep", "tp"), None),
            P(("grp", "ep", "tp"), None),
            P(("grp", "ep", "tp"), None),
            P(),
            P("tp", None),
            P(("grp", "ep", "tp"), None),
            P(),
            P(("grp", "ep", "tp"), None),
            P(("grp", "ep", "tp"), None),
            P("ep", None, "tp"),
            P("ep", None, "tp"),
            P("ep", "tp", None),
        ),
        out_specs=(P(("grp", "ep", "tp"), None), P(("grp", "ep", "tp"), None)),
        check_vma=False,
    )
```

profile of v0, /device:TPU:0, one launch (start us, length us, event | category | flops | bytes accessed | tf_op | source)
XLA Modules:
  0.0 306.5 jit_solution(13236380479870054921)
XLA Ops:
  7.2 0.9 copy.24
  8.2 0.1 eq.25
  8.4 1.2 reduce-window.6
  10.2 0.7 compare_select_fusion.2
  11.4 1.4 scatter_custom_fusion
  12.8 1.2 fusion.2
  14.0 1.2 fusion.4
  15.3 3.3 %gather_fusion = bf16[512,2048]{1,0:T(8,128)(2,1)} fusion(bf16[129,2048]{1,0:T(8,128)(2,1)S(1)} %concatenate.7, s32[1024]{0:T(1024)S(1)} %pad_clamp_fusion.1), kind=kCustom, calls=%fused_computation | custom fusion | bytes 4196352 | tf_op jit(solution)/shard_map/gather | solution.py:81
  18.6 54.6 %all_to_all.24 = bf16[4,128,2048]{2,1,0:T(8,128)(2,1)} all-to-all(bf16[4,128,2048]{2,1,0:T(8,128)(2,1)} %bitcast.41), channel_id=1, replica_groups=mesh['grp'=2,'ep'=4,'tp'=4] {'ep'}, dimensions={0} | all-to-all | bytes 4194304 | tf_op jit(solution)/shard_map/all_to_all | solution.py:82
  73.4 57.6 %all-gather.5.cloned.1.call-done = bf16[2048,2048]{1,0:T(8,128)(2,1)} async-done(((bf16[512,2048]{1,0:T(8,128)(2,1)}), bf16[2048,2048]{1,0:T(8,128)(2,1)}) %all-gather.5.cloned.1.call-update) | async-done | bytes 8388624 | tf_op jit(solution)/shard_map/all_gather | solution.py:84
  130.9 7.1 %fusion.9 = f32[2048,256]{1,0:T(8,128)} fusion(bf16[2048,2048]{1,0:T(8,128)(2,1)} %all-gather.5.cloned.1.call-done, bf16[1,2048,256]{2,1,0:T(8,128)(2,1)S(1)} %copy-done.4), kind=kOutput, calls=%fused_computation.22 | convolution fusion | flops 2147483648 | bytes 11534336 | tf_op jit(solution)/shard_map/dot_general | solution.py:30
  138.0 13.2 %convolution_convert_fusion = bf16[2048,2048]{1,0:T(8,128)(2,1)} fusion(bf16[2048,2048]{1,0:T(8,128)(2,1)} %all-gather.5.cloned.1.call-done, f32[2048,256]{1,0:T(8,128)} %fusion.9, bf16[1,256,2048]{2,1,0:T(8,128)(2,1)S(1)} %copy-done, bf16[1,2048,256]{2,1,0:T(8,128)(2,1)S(1)} %copy-done.5), kind=kOutput, calls=%fused_computation.3 | convolution fusion | flops 4302307328 | bytes 20971520 | tf_op jit(solution)/shard_map/dot_general | solution.py:87
  151.3 0.7 all-gather.3.cloned.1.call-update
  152.0 70.8 %reduce-scatter.2.cloned.1.call-done = bf16[512,2048]{1,0:T(8,128)(2,1)} async-done(((bf16[2048,2048]{1,0:T(8,128)(2,1)}), bf16[512,2048]{1,0:T(8,128)(2,1)}) %reduce-scatter.2.cloned.1.call-update) | async-done | bytes 2097168 | tf_op jit(solution)/shard_map/reduce_scatter | solution.py:86
  222.8 4.6 %all-to-all-start.1 = ((bf16[4,128,2048]{2,1,0:T(8,128)(2,1)}), bf16[4,128,2048]{2,1,0:T(8,128)(2,1)S(1)}, u32[]{:S(2)}, u32[]{:S(2)}) async-start(bf16[4,128,2048]{2,1,0:T(8,128)(2,1)} %bitcast.43), calls=%async_computation.2 | async-start | bytes 4194304 | tf_op jit(solution)/shard_map/all_to_all | solution.py:92
  227.4 1.9 multiply_convert_fusion.1
  229.3 1.0 copy-done.1
  230.3 1.5 collective-permute-start
  232.3 0.2 collective-permute-done
  232.5 50.2 %all-gather.3.cloned.1.call-done = bf16[2048,2048]{1,0:T(8,128)(2,1)} async-done(((bf16[512,2048]{1,0:T(8,128)(2,1)}), bf16[2048,2048]{1,0:T(8,128)(2,1)}) %all-gather.3.cloned.1.call-update) | async-done | bytes 8388624 | tf_op jit(solution)/shard_map/all_gather | solution.py:62
  282.7 8.6 %convolution_convert_fusion.1 = bf16[256,2048]{1,0:T(8,128)(2,1)} fusion(bf16[2048,2048]{1,0:T(8,128)(2,1)} %all-gather.3.cloned.1.call-done, bf16[256,2048]{1,0:T(8,128)(2,1)} %copy-done.1, bf16[256,2048]{1,0:T(8,128)(2,1)} %param.14, bf16[2,2048]{1,0:T(2,128)(2,1)S(1)} %collective-permute-done, f32[2048]{0:T(1024)S(1)} %bitcast.45, f32[2048]{0:T(1024)S(1)} %bitcast.46, ...), kind=kOutput, calls=%fused_computation.6 | convolution fusion | flops 2156920832 | bytes 11567104 | tf_op jit(solution)/shard_map/dot_general | solution.py:60
  291.3 2.3 gather_fusion.1
  293.6 2.4 reshape.104
  296.0 3.9 %multiply_reduce_fusion = bf16[128,2048]{1,0:T(8,128)(2,1)} fusion(f32[128,2,2048]{2,1,0:T(2,128)S(1)} %reshape.104, f32[128,2]{1,0:T(8,128)S(1)} %copy.31), kind=kLoop, calls=%fused_computation.7 | loop fusion | flops 786432 | bytes 2622464 | tf_op jit(solution)/shard_map/reduce_sum | solution.py:95
  (45 shorter events, 1.8 us)
Async XLA Ops:
  7.2 130.9 %copy-start = (bf16[1,256,2048]{2,1,0:T(8,128)(2,1)S(1)}, bf16[1,256,2048]{2,1,0:T(8,128)(2,1)}, u32[]{:S(2)}) copy-start(bf16[1,256,2048]{2,1,0:T(8,128)(2,1)} %param.23) | copy-start | bytes 3145732
  7.2 123.8 %all-gather.5.cloned.1.call-start = ((), (), s32[]{:S(2)}) async-start(), calls=%async_computation.4 | async-start | bytes 10485760 | tf_op jit(solution)/shard_map/all_gather | solution.py:84
  73.3 57.7 %copy-start.4 = (bf16[1,2048,256]{2,1,0:T(8,128)(2,1)S(1)}, bf16[1,2048,256]{2,1,0:T(8,128)(2,1)}, u32[]{:S(2)}) copy-start(bf16[1,2048,256]{2,1,0:T(8,128)(2,1)} %param.21) | copy-start | bytes 3145732
  73.3 64.7 %copy-start.5 = (bf16[1,2048,256]{2,1,0:T(8,128)(2,1)S(1)}, bf16[1,2048,256]{2,1,0:T(8,128)(2,1)}, u32[]{:S(2)}) copy-start(bf16[1,2048,256]{2,1,0:T(8,128)(2,1)} %param.22) | copy-start | bytes 3145732
  73.3 149.5 %reduce-scatter.2.cloned.1.call-start = ((), (), s32[]{:S(2)}) async-start(), calls=%async_computation.5 | async-start | bytes 10485760 | tf_op jit(solution)/shard_map/reduce_scatter | solution.py:86
  151.2 131.4 %all-gather.3.cloned.1.call-start = ((), (), s32[]{:S(2)}) async-start(), calls=%async_computation.3 | async-start | bytes 10485760 | tf_op jit(solution)/shard_map/all_gather | solution.py:62
  222.8 68.5 %all-to-all-start.1 = ((bf16[4,128,2048]{2,1,0:T(8,128)(2,1)}), bf16[4,128,2048]{2,1,0:T(8,128)(2,1)S(1)}, u32[]{:S(2)}, u32[]{:S(2)}) async-start(bf16[4,128,2048]{2,1,0:T(8,128)(2,1)} %bitcast.43), calls=%async_computation.2 | async-start | bytes 4194304 | tf_op jit(solution)/shard_map/all_to_all | solution.py:92
  227.4 4.7 %copy-start.3 = (f32[128,2]{0,1:T(2,128)S(1)}, f32[128,2]{0,1:T(2,128)}, u32[]{:S(2)}) copy-start(f32[128,2]{0,1:T(2,128)} %param.20) | copy-start | bytes 3076
  227.4 4.8 %copy-start.2 = (f32[3,2048]{1,0:T(4,128)S(1)}, f32[3,2048]{1,0:T(4,128)}, u32[]{:S(2)}) copy-start(f32[3,2048]{1,0:T(4,128)} %param.15) | copy-start | bytes 73732
  229.3 1.0 copy-start.1
  230.3 2.1 collective-permute-start
Sparse Core Ops, SparseCore 0:
  73.4 57.4 all-gather.4
  151.3 71.3 reduce-scatter.1
  224.3 58.2 all-gather.2
where the time goes:
time: 307 us; the launch traced here: 306 us
  waiting for transfers between devices  179 us (58%)
  blocking collectives  54.6 us (18%)
  matrix products  28.9 us (9%)
  between operations  13.9 us (5%)
  local copies, waits for them, and re-layouts  12.9 us (4%)
  other arithmetic  10.5 us (3%)
  starting transfers between devices  6.22 us (2%)
    reduce_scatter x1, waiting for transfers between devices, per_device(): lax.psum_scatter(jnp.dot(hidden, weight_down, preferred_element_type=jnp....  70.8 us
    all_gather x1, waiting for transfers between devices, per_device(): lax.all_gather(arrived, 'tp', axis=0, tiled=True)  57.6 us
    all_to_all x1, blocking collectives, per_device(): lax.all_to_all(outgoing, 'ep', split_axis=0, concat_axis=0, tiled=True)  54.6 us
    all_gather x1, waiting for transfers between devices, per_device(): lax.all_gather(w_out, 'tp', axis=0, tiled=True)  50.2 us
    dot_general x1, matrix products, per_device(): jnp.dot(hidden, weight_down, preferred_element_type=jnp.float32)  13.2 us
    dot_general x1, matrix products, per_device(): jnp.dot(gated_rows, lax.all_gather(w_out, 'tp', axis=0, tiled=True), pref...  8.61 us
    dot_general x1, matrix products, expert_hidden(): gate_val = jnp.dot(rows, weight_gate, preferred_element_type=jnp.float32)  7.09 us
  transfers between devices with their start and end apart: 5, of which 4 were waited for; matrix products, arithmetic and copies ran while one was open for 4% of the time, Pallas kernels for 0%

commit v1 on v0

--- a/solution.py
+++ b/solution.py
@@ -1,6 +1,9 @@
+import functools
 import jax
 import jax.numpy as jnp
 from jax import lax
+from jax.experimental import pallas as pl
+from jax.experimental.pallas import tpu as pltpu
 from jax.sharding import PartitionSpec as P
 
 D = 2048
@@ -30,6 +33,407 @@
     gate_val = jnp.dot(rows, weight_gate, preferred_element_type=jnp.float32)
     up_val = jnp.dot(rows, weight_up, preferred_element_type=jnp.float32)
     return (jax.nn.silu(gate_val) * up_val).astype(jnp.bfloat16)
+
+
+F32 = jnp.float32
+BF16 = jnp.bfloat16
+
+
+def fused_kernel(
+    conv_x, conv_c, conv_b, taps, w_out, tokens, gain, coef, w_gate, w_up, w_down,
+    mixed_ref, experts_ref,
+    full_g, full_u, full_d, full_o, tok, normed, cf, hidden, contrib,
+    in_l, in_r, out_l, out_r, cx, cc, cb, hx, hc, ext, gated,
+    x_s, x_r, y_s, y_r, dx_s, dx_r, dy_s, dy_r, own_s, own_r,
+    zr_s, zr_r, zl_s, zl_r, cf_s, cf_r, h_s, h_r, rl_s, rl_r, rr_s, rr_r, loc,
+):
+    n_ep, rows, width = tok.shape
+    half = rows // 2
+    rows_mix = cx.shape[0]
+    edge = hx.shape[0]
+    last_z = n_ep - 1
+    y = lax.axis_index("grp")
+    z = lax.axis_index("ep")
+    k = lax.axis_index("tp")
+    n_tp = full_g.shape[0]
+    core = lax.rem(k, 2)
+    mate = k + 1 - 2 * core
+    far = lax.rem(k + 2, n_tp)
+    far_mate = lax.rem(mate + 2, n_tp)
+    other_y = 1 - y
+    flat = z * n_tp + k
+    total = n_ep * n_tp
+    nxt = lax.rem(flat + 1, total)
+    prv = lax.rem(flat + total - 1, total)
+    nxt_id = {"ep": lax.div(nxt, n_tp), "tp": lax.rem(nxt, n_tp)}
+    prv_id = {"ep": lax.div(prv, n_tp), "tp": lax.rem(prv, n_tp)}
+
+    def rc(src, dst, send, recv, dev):
+        return pltpu.make_async_remote_copy(
+            src_ref=src, dst_ref=dst, send_sem=send, recv_sem=recv,
+            device_id=dev, device_id_type=pl.DeviceIdType.MESH,
+        )
+
+    locals_ = [
+        (tokens, tok.at[z]), (coef, cf.at[z]),
+        (conv_x, cx), (conv_c, cc), (conv_b, cb),
+        (w_gate.at[0], full_g.at[k]), (w_up.at[0], full_u.at[k]),
+        (w_down.at[0], full_d.at[k]), (w_out, full_o.at[k]),
+    ]
+    local_copies = [pltpu.make_async_copy(a, b, loc.at[i]) for i, (a, b) in enumerate(locals_)]
+    for cp in local_copies:
+        cp.start()
+
+    barrier = pltpu.get_barrier_semaphore()
+    peers = [{"tp": mate}, {"tp": far}, {"grp": other_y}, nxt_id, prv_id]
+    peers += [{"ep": lax.rem(z + m, n_ep)} for m in range(1, n_ep)]
+    for dev in peers:
+        pl.semaphore_signal(barrier, inc=1, device_id=dev, device_id_type=pl.DeviceIdType.MESH)
+    pl.semaphore_wait(barrier, len(peers))
+
+    pieces = [(w_gate.at[0], full_g, 2), (w_up.at[0], full_u, 2), (w_down.at[0], full_d, 2), (w_out, full_o, 4)]
+    chunks = []
+    for own, full, cuts in pieces:
+        per_half = full.shape[1] // 2
+        size = per_half // cuts
+        for j in range(cuts):
+            chunks.append((own, full, per_half, size, j))
+    n_chunks = len(chunks)
+
+    def span(i, h):
+        _, _, per_half, size, j = chunks[i]
+        return pl.ds(pl.multiple_of(h * per_half + j * size, size), size)
+
+    def x_copy(i):
+        own, full = chunks[i][:2]
+        return rc(own.at[span(i, y)], full.at[k, span(i, y)], x_s.at[i], x_r.at[i], {"tp": far})
+
+    def y_copy(i):
+        at = chunks[i][1].at[far, span(i, y)]
+        return rc(at, at, y_s.at[i], y_r.at[i], {"grp": other_y})
+
+    def dx_copy(i):
+        at = chunks[i][1].at[far, span(i, y)]
+        return rc(at, at, dx_s.at[i], dx_r.at[i], {"tp": mate})
+
+    def dy_copy(i):
+        at = chunks[i][1].at[far, span(i, other_y)]
+        return rc(at, at, dy_s.at[i], dy_r.at[i], {"tp": mate})
+
+    def own_copy(i):
+        own, full, _ = pieces[i]
+        return rc(own, full.at[k], own_s.at[i], own_r.at[i], {"tp": mate})
+
+    def got(i, piece, h, send, recv):
+        at = chunks[i][1].at[piece, span(i, h)]
+        rc(at, at, send.at[i], recv.at[i], {"tp": mate}).wait_recv()
+
+    rows_of = lambda j: pl.ds((j % 2) * half, half)
+
+    def zr_send(j):
+        b = z - j // 2
+        src = tokens.at[rows_of(j)] if j < 2 else tok.at[b, rows_of(j)]
+        return rc(src, tok.at[b, rows_of(j)], zr_s.at[j], zr_r.at[j], {"ep": z + 1})
+
+    def zl_send(j):
+        b = z + j // 2
+        src = tokens.at[rows_of(j)] if j < 2 else tok.at[b, rows_of(j)]
+        return rc(src, tok.at[b, rows_of(j)], zl_s.at[j], zl_r.at[j], {"ep": z - 1})
+
+    def zr_got(j):
+        at = tok.at[z - 1 - j // 2, rows_of(j)]
+        rc(at, at, zr_s.at[j], zr_r.at[j], {"ep": z - 1}).wait_recv()
+
+    def zl_got(j):
+        at = tok.at[z + 1 + j // 2, rows_of(j)]
+        rc(at, at, zl_s.at[j], zl_r.at[j], {"ep": z + 1}).wait_recv()
+
+    def cf_copy(m):
+        return rc(coef, cf.at[z], cf_s.at[m - 1], cf_r.at[m - 1], {"ep": lax.rem(z + m, n_ep)})
+
+    tail = pl.ds(rows_mix - edge, edge)
+
+    def halo_copies():
+        return (
+            rc(conv_x.at[tail], hx, h_s.at[0], h_r.at[0], nxt_id),
+            rc(conv_c.at[tail], hc, h_s.at[1], h_r.at[1], nxt_id),
+        )
+
+    is_first, is_last = flat == 0, flat == total - 1
+
+    for m in range(1, n_ep):
+        cf_copy(m).start()
+
+    @pl.when(jnp.logical_not(is_last))
+    def _():
+        for cp in halo_copies():
+            cp.start()
+
+    for j in range(2):
+        pl.when(z < last_z)(lambda j=j: zr_send(j).start())
+        pl.when(z > 0)(lambda j=j: zl_send(j).start())
+    for i in range(n_chunks):
+        x_copy(i).start()
+    for i in range(len(pieces)):
+        own_copy(i).start()
+    for cp in local_copies:
+        cp.wait()
+
+    @pl.when(is_first)
+    def _():
+        hx[...] = jnp.zeros_like(hx)
+        hc[...] = jnp.zeros_like(hc)
+
+    @pl.when(jnp.logical_not(is_first))
+    def _():
+        for cp in halo_copies():
+            cp.wait_recv()
+
+    n_taps = taps.shape[0]
+
+    def conv_tile(t, _):
+        cols = pl.ds(pl.multiple_of(t * 128, 128), 128)
+        ext[pl.ds(0, edge), :] = (hc[:, cols].astype(F32) * hx[:, cols].astype(F32)).astype(BF16).astype(F32)
+        ext[pl.ds(edge, rows_mix), :] = (cc[:, cols].astype(F32) * cx[:, cols].astype(F32)).astype(BF16).astype(F32)
+        filtered = jnp.zeros((rows_mix, 128), F32)
+        for s in range(n_taps):
+            filtered = filtered + taps[pl.ds(s, 1), cols] * ext[pl.ds(edge - (n_taps - 1) + s, rows_mix), :]
+        gated[:, cols] = (cb[:, cols].astype(F32) * filtered).astype(BF16)
+        return 0
+
+    lax.fori_loop(0, cx.shape[1] // 128, conv_tile, 0)
+
+    def norm_block(b):
+        def body(r, _):
+            at = pl.ds(pl.multiple_of(r * 32, 32), 32)
+            v = tok[b, at, :].astype(F32)
+            scale = lax.rsqrt(jnp.mean(v * v, axis=-1, keepdims=True) + 1e-06)
+            normed[pl.ds(pl.multiple_of(b * rows + r * 32, 32), 32), :] = (v * scale * gain[...]).astype(BF16)
+            return 0
+
+        lax.fori_loop(0, rows // 32, body, 0)
+
+    norm_block(z)
+
+    def weight_step(i):
+        if i < n_chunks:
+            got(i, far, y, x_s, x_r)
+            y_copy(i).start()
+            dx_copy(i).start()
+        if 1 <= i <= n_chunks:
+            got(i - 1, far, other_y, y_s, y_r)
+            dy_copy(i - 1).start()
+
+    def mate_wait(lo, hi):
+        for i in range(lo, hi):
+            got(i, far_mate, y, dx_s, dx_r)
+            got(i, far_mate, other_y, dy_s, dy_r)
+
+    def own_wait(i):
+        at = pieces[i][1].at[mate]
+        rc(at, at, own_s.at[i], own_r.at[i], {"tp": mate}).wait_recv()
+
+    steps = 2 * last_z
+    for s in range(steps):
+        @pl.when(s < 2 * z)
+        def _():
+            zr_got(s)
+            if s + 2 < steps:
+                pl.when(z < last_z)(lambda: zr_send(s + 2).start())
+
+        @pl.when(s < 2 * (last_z - z))
+        def _():
+            zl_got(s)
+            if s + 2 < steps:
+                pl.when(z > 0)(lambda: zl_send(s + 2).start())
+
+        weight_step(s)
+        if s % 2 == 1:
+            m = s // 2 + 1
+            pl.when(z - m >= 0)(lambda: norm_block(z - m))
+            pl.when(z + m <= last_z)(lambda: norm_block(z + m))
+
+    mate_wait(0, 4)
+    own_wait(0)
+    own_wait(1)
+
+    def hidden_piece(p, _):
+        g = jnp.dot(normed[...], full_g[p], preferred_element_type=F32)
+        u = jnp.dot(normed[...], full_u[p], preferred_element_type=F32)
+        hidden[p] = (jax.nn.silu(g) * u).astype(BF16)
+        return 0
+
+    lax.fori_loop(0, n_tp, hidden_piece, 0)
+    weight_step(6)
+    mate_wait(4, 6)
+    own_wait(2)
+    for m in range(1, n_ep):
+        at = cf.at[lax.rem(z + n_ep - m, n_ep)]
+        rc(at, at, cf_s.at[m - 1], cf_r.at[m - 1], {"ep": z}).wait_recv()
+
+    eye = lax.broadcasted_iota(jnp.int32, (rows, rows), 0) == lax.broadcasted_iota(jnp.int32, (rows, rows), 1)
+    columns = []
+    for b in range(n_ep):
+        line = cf[b, pl.ds(z, 1), :]
+        columns.append(jnp.sum(jnp.where(eye, jnp.broadcast_to(line, (rows, rows)), 0.0), axis=1, keepdims=True))
+    column = jnp.concatenate(columns, axis=0)
+    tile = 256
+
+    def down_tile(t, _):
+        cols = pl.ds(pl.multiple_of(t * tile, tile), tile)
+        acc = jnp.dot(hidden[0], full_d[0, :, cols], preferred_element_type=F32)
+        for p in range(1, n_tp):
+            acc = acc + jnp.dot(hidden[p], full_d[p, :, cols], preferred_element_type=F32)
+        contrib[:, cols] = acc * column
+        return 0
+
+    lax.fori_loop(0, width // tile, down_tile, 0)
+
+    def own_rows(d, h):
+        return contrib[pl.ds(pl.multiple_of(d * rows + h * half, half), half), :]
+
+    def rl_copy(s):
+        return rc(out_l.at[s], in_l.at[s], rl_s.at[s], rl_r.at[s], {"ep": z - 1})
+
+    def rr_copy(s):
+        return rc(out_r.at[s], in_r.at[s], rr_s.at[s], rr_r.at[s], {"ep": z + 1})
+
+    def rl_got(s):
+        rc(in_l.at[s], in_l.at[s], rl_s.at[s], rl_r.at[s], {"ep": z}).wait_recv()
+
+    def rr_got(s):
+        rc(in_r.at[s], in_r.at[s], rr_s.at[s], rr_r.at[s], {"ep": z}).wait_recv()
+
+    def side(s, depth, inbox, outbox, got_fn, copy_fn, dest_fn):
+        has_in = depth < last_z
+
+        @pl.when(jnp.logical_and(s >= 0, jnp.logical_and(has_in, s < 2 * (depth + 1))))
+        def _():
+            got_fn(s)
+
+        @pl.when(jnp.logical_and(s >= 0, s < 2 * depth))
+        def _():
+            mine = own_rows(dest_fn(lax.div(s, 2)), lax.rem(s, 2))
+
+            @pl.when(has_in)
+            def _():
+                outbox[s] = (mine + inbox[s].astype(F32)).astype(BF16)
+
+            @pl.when(jnp.logical_not(has_in))
+            def _():
+                outbox[s] = mine.astype(BF16)
+
+            copy_fn(s).start()
+
+    for t in range(steps + 1):
+        if t == steps:
+            mate_wait(6, n_chunks)
+            own_wait(3)
+
+            def mixed_tile(q, _):
+                cols = pl.ds(pl.multiple_of(q * tile, tile), tile)
+                part = full_o.shape[1]
+                acc = jnp.zeros((rows_mix, tile), F32)
+                for p in range(n_tp):
+                    acc = acc + jnp.dot(gated[:, p * part : (p + 1) * part], full_o[p, :, cols], preferred_element_type=F32)
+                mixed_ref[:, cols] = acc.astype(BF16)
+                return 0
+
+            lax.fori_loop(0, width // tile, mixed_tile, 0)
+        side(t - (last_z - z), z, in_l, out_l, rl_got, rl_copy, lambda b: b)
+        side(t - z, last_z - z, in_r, out_r, rr_got, rr_copy, lambda b: last_z - b)
+        if 7 + t <= n_chunks:
+            weight_step(7 + t)
+
+    for h in range(2):
+        at = pl.ds(h * half, half)
+        mine = own_rows(z, h)
+
+        @pl.when(z == 0)
+        def _():
+            experts_ref[at, :] = (mine + in_l[h].astype(F32)).astype(BF16)
+
+        @pl.when(z == last_z)
+        def _():
+            experts_ref[at, :] = (mine + in_r[h].astype(F32)).astype(BF16)
+
+        @pl.when(jnp.logical_and(z > 0, z < last_z))
+        def _():
+            experts_ref[at, :] = (
+                mine + in_l[2 * z + h].astype(F32) + in_r[2 * (last_z - z) + h].astype(F32)
+            ).astype(BF16)
+
+    for i in range(n_chunks):
+        x_copy(i).wait_send()
+        y_copy(i).wait_send()
+        dx_copy(i).wait_send()
+        dy_copy(i).wait_send()
+    for i in range(len(pieces)):
+        own_copy(i).wait_send()
+    for m in range(1, n_ep):
+        cf_copy(m).wait_send()
+
+    @pl.when(jnp.logical_not(is_last))
+    def _():
+        for cp in halo_copies():
+            cp.wait_send()
+
+    for j in range(steps):
+        pl.when(jnp.logical_and(z < last_z, j < 2 * (z + 1)))(lambda j=j: zr_send(j).wait_send())
+        pl.when(jnp.logical_and(z > 0, j < 2 * (last_z - z + 1)))(lambda j=j: zl_send(j).wait_send())
+        pl.when(j < 2 * z)(lambda j=j: rl_copy(j).wait_send())
+        pl.when(j < 2 * (last_z - z))(lambda j=j: rr_copy(j).wait_send())
+
+
+def per_device_fused(
+    conv_x, conv_c, conv_b, conv_taps, w_out, tokens_b, norm_gain,
+    route_b, route_weights, w_gate, w_up, w_down,
+):
+    n_ep, n_tp = lax.axis_size("ep"), lax.axis_size("tp")
+    rows, width = tokens_b.shape
+    rows_mix, channels = conv_x.shape
+    hid = w_gate.shape[2]
+    shares = route_weights / jnp.sum(route_weights, axis=-1, keepdims=True)
+    lanes = jnp.arange(-(-n_ep // 8) * 8, dtype=jnp.int32)[:, None, None]
+    coef = jnp.sum(jnp.where(route_b.T[None] == lanes, shares.T[None], 0.0), axis=1)
+    edge, half, steps = 16, rows // 2, 2 * (n_ep - 1)
+    n_chunks = 10
+    dma = pltpu.SemaphoreType.DMA
+    hbm, vmem = pl.BlockSpec(memory_space=pl.ANY), pl.BlockSpec(memory_space=pltpu.VMEM)
+    return pl.pallas_call(
+        fused_kernel,
+        out_shape=(
+            jax.ShapeDtypeStruct((rows_mix, width), BF16),
+            jax.ShapeDtypeStruct((rows, width), BF16),
+        ),
+        in_specs=[hbm, hbm, hbm, vmem, hbm, hbm, vmem, hbm, hbm, hbm, hbm],
+        out_specs=(vmem, vmem),
+        scratch_shapes=[
+            pltpu.VMEM((n_tp,) + w_gate.shape[1:], BF16),
+            pltpu.VMEM((n_tp,) + w_up.shape[1:], BF16),
+            pltpu.VMEM((n_tp,) + w_down.shape[1:], BF16),
+            pltpu.VMEM((n_tp,) + w_out.shape, BF16),
+            pltpu.VMEM((n_ep, rows, width), BF16),
+            pltpu.VMEM((n_ep * rows, width), BF16),
+            pltpu.VMEM((n_ep,) + coef.shape, F32),
+            pltpu.VMEM((n_tp, n_ep * rows, hid), BF16),
+            pltpu.VMEM((n_ep * rows, width), F32),
+        ]
+        + [pltpu.VMEM((steps, half, width), BF16)] * 4
+        + [pltpu.VMEM((rows_mix, channels), BF16)] * 3
+        + [pltpu.VMEM((edge, channels), BF16)] * 2
+        + [pltpu.VMEM((edge + rows_mix, 128), F32), pltpu.VMEM((rows_mix, channels), BF16)]
+        + [dma((n_chunks,))] * 8
+        + [dma((4,))] * 2
+        + [dma((steps,))] * 4
+        + [dma((n_ep - 1,))] * 2
+        + [dma((2,))] * 2
+        + [dma((steps,))] * 4
+        + [dma((9,))],
+        compiler_params=pltpu.CompilerParams(
+            collective_id=0, has_side_effects=True, vmem_limit_bytes=62 * 1024 * 1024
+        ),
+    )(conv_x, conv_c, conv_b, conv_taps, w_out, tokens_b, norm_gain[None], coef, w_gate, w_up, w_down)
 
 
 def per_device(
@@ -99,8 +503,9 @@
 
 
 def solution(mesh):
+    dense = mesh.shape["ep"] <= 2 * TOPK and mesh.shape["tp"] == 4 and mesh.shape["grp"] == 2
     return jax.shard_map(
-        per_device,
+        per_device_fused if dense else per_device,
         mesh=mesh,
         in_specs=(
             P(("grp", "ep", "tp"), None),

time: 307 us -> 101 us (0.33)
  waiting for transfers between devices: 179 us -> 0 us
  Pallas kernels: 0 us -> 94.1 us
  blocking collectives: 54.6 us -> 0 us
  matrix products: 28.9 us -> 0 us
  between operations: 13.9 us -> 0.65 us
  local copies, waits for them, and re-layouts: 12.9 us -> 3.16 us
  other arithmetic: 10.5 us -> 2.66 us
  starting transfers between devices: 6.22 us -> 0 us
    all_gather x2 -> x0, waiting for transfers between devices: 108 us -> none  [the longest x1 57.6 us: per_device(): lax.all_gather(arrived, 'tp', axis=0, tiled=True)]
    pallas_call x0 -> x1, Pallas kernels: none -> 94.1 us  [per_device_fused(): pl.pallas_call(fused_kernel, out_shape=(jax.ShapeDtypeStruct((rows_mix, w...]
    reduce_scatter x1 -> x0, waiting for transfers between devices: 70.8 us -> none  [per_device(): lax.psum_scatter(jnp.dot(hidden, weight_down, preferred_element_type=jnp....]
    all_to_all x1 -> x0, blocking collectives: 54.6 us -> none  [per_device(): lax.all_to_all(outgoing, 'ep', split_axis=0, concat_axis=0, tiled=True)]
    dot_general x3 -> x0, matrix products: 28.9 us -> none  [the longest x1 13.2 us: per_device(): jnp.dot(hidden, weight_down, preferred_element_type=jnp.float32)]
    gather x2 -> x0, local copies, waits for them, and re-layouts: 5.64 us -> none  [the longest x1 3.29 us: per_device(): outgoing = padded_rows[fill_slots(targets, slot_total, rows_exp)]]
    all_to_all x1 -> x0, starting transfers between devices: 4.6 us -> none  [per_device(): lax.all_to_all(summed, 'ep', split_axis=0, concat_axis=0, tiled=True)]
    reduce_sum x4 -> x2, other arithmetic: 5.2 us -> 1.98 us  [the longest x1 1.28 us: per_device_fused(): jnp.sum(jnp.where(route_b.T[None] == lanes, shares.T[None], 0.0), axis=1)]
  transfers between devices with their start and end apart: 5 -> 0, of which waited for: 4 -> 0; matrix products, arithmetic and copies ran while one was open for 4% -> 0% of each run, Pallas kernels for 0% -> 0%
where the time goes in v1:
time: 101 us
  Pallas kernels  94.1 us (93%)
  local copies, waits for them, and re-layouts  3.16 us (3%)
  other arithmetic  2.66 us (3%)
    pallas_call x1, Pallas kernels, per_device_fused(): pl.pallas_call(fused_kernel, out_shape=(jax.ShapeDtypeStruct((rows_mix, w...  94.1 us
    unnamed x4, local copies, waits for them, and re-layouts  3.16 us

profile of v1, /device:TPU:0, one launch (start us, length us, event | category | flops | bytes accessed | tf_op | source)
XLA Modules:
  0.0 100.6 jit_solution(3782864788720833059)
XLA Ops:
  0.6 0.7 reduce_sum.18
  1.3 0.7 divide_bitcast_fusion
  2.0 1.3 %select_reduce_fusion.coef = f32[8,128]{1,0:T(8,128)} fusion(f32[2,128]{1,0:T(2,128)S(1)} %divide_bitcast_fusion, s32[2,128]{1,0:T(2,128)} %bitcast.5), kind=kLoop, calls=%fused_computation | loop fusion | flops 5120 | bytes 6144 | tf_op jit(solution)/shard_map/reduce_sum | solution.py:398
  3.3 94.1 %shard_map.131 = (bf16[256,2048]{1,0:T(8,128)(2,1)}, bf16[128,2048]{1,0:T(8,128)(2,1)}) custom-call(bf16[256,2048]{1,0:T(8,128)(2,1)} %conv_x.1, bf16[256,2048]{1,0:T(8,128)(2,1)} %conv_c.1, bf16[256,2048]{1,0:T(8,128)(2,1)} %conv_b.1, f32[3,2048]{1,0:T(4,128)} %taps.1, bf16[512,2048]{1,0:T(8,128)(2,1)} %w_out.1, bf16[128,2048]{1,0:T(8,128)(2,1)} %tokens.1, ...), custom_call_target="tpu_custom_call" | custom-call | tf_op jit(solution)/shard_map/pallas_call | solution.py:403
  97.4 0.0 copy-start
  97.4 2.4 %copy.16 = bf16[256,2048]{1,0:T(8,128)(2,1)} copy(bf16[256,2048]{1,0:T(8,128)(2,1)} %get-tuple-element.4) | data formatting | bytes 2097152
  99.8 0.0 copy-done
  99.8 0.8 copy.17
Async XLA Ops:
  97.4 2.4 %copy-start = (bf16[128,2048]{1,0:T(8,128)(2,1)S(1)}, bf16[128,2048]{1,0:T(8,128)(2,1)}, u32[]{:S(2)}) copy-start(bf16[128,2048]{1,0:T(8,128)(2,1)} %get-tuple-element.5) | copy-start | bytes 1572868

commit v2 on v1

--- a/solution.py
+++ b/solution.py
@@ -37,15 +37,16 @@
 
 F32 = jnp.float32
 BF16 = jnp.bfloat16
+CUTS = ((2, (1,)), (2, (1,)), (1, (2, 1)), (4, (1,)))
 
 
 def fused_kernel(
-    conv_x, conv_c, conv_b, taps, w_out, tokens, gain, coef, w_gate, w_up, w_down,
+    conv_x, conv_c, conv_b, taps, w_out, tokens, gain, route, weights, w_gate, w_up, w_down,
     mixed_ref, experts_ref,
-    full_g, full_u, full_d, full_o, tok, normed, cf, hidden, contrib,
+    full_g, full_u, full_d, full_o, tok, normed, rt, wt, hidden, contrib,
     in_l, in_r, out_l, out_r, cx, cc, cb, hx, hc, ext, gated,
     x_s, x_r, y_s, y_r, dx_s, dx_r, dy_s, dy_r, own_s, own_r,
-    zr_s, zr_r, zl_s, zl_r, cf_s, cf_r, h_s, h_r, rl_s, rl_r, rr_s, rr_r, loc,
+    zr_s, zr_r, zl_s, zl_r, rt_s, rt_r, wt_s, wt_r, h_s, h_r, rl_s, rl_r, rr_s, rr_r, loc,
 ):
     n_ep, rows, width = tok.shape
     half = rows // 2
@@ -75,7 +76,7 @@
         )
 
     locals_ = [
-        (tokens, tok.at[z]), (coef, cf.at[z]),
+        (tokens, tok.at[z]), (route, rt.at[z]), (weights, wt.at[z]),
         (conv_x, cx), (conv_c, cc), (conv_b, cb),
         (w_gate.at[0], full_g.at[k]), (w_up.at[0], full_u.at[k]),
         (w_down.at[0], full_d.at[k]), (w_out, full_o.at[k]),
@@ -91,41 +92,47 @@
         pl.semaphore_signal(barrier, inc=1, device_id=dev, device_id_type=pl.DeviceIdType.MESH)
     pl.semaphore_wait(barrier, len(peers))
 
-    pieces = [(w_gate.at[0], full_g, 2), (w_up.at[0], full_u, 2), (w_down.at[0], full_d, 2), (w_out, full_o, 4)]
+    pieces = [(w_gate.at[0], full_g), (w_up.at[0], full_u), (w_down.at[0], full_d), (w_out, full_o)]
+    out_cols = full_d.shape[2] // 2
     chunks = []
-    for own, full, cuts in pieces:
-        per_half = full.shape[1] // 2
-        size = per_half // cuts
-        for j in range(cuts):
-            chunks.append((own, full, per_half, size, j))
+    for at, (rows_cut, cols_cut) in enumerate(CUTS):
+        half_rows, cols = pieces[at][1].shape[1] // 2, pieces[at][1].shape[2]
+        for c, cuts in enumerate(cols_cut):
+            for j in range(rows_cut * cuts):
+                size = half_rows // (rows_cut * cuts)
+                wide = cols // len(cols_cut)
+                chunks.append((at, j * size, size, c * wide, wide))
     n_chunks = len(chunks)
 
-    def span(i, h):
-        _, _, per_half, size, j = chunks[i]
-        return pl.ds(pl.multiple_of(h * per_half + j * size, size), size)
+    def part(i, ref, h):
+        at, first, size, col, wide = chunks[i]
+        start = pl.multiple_of(h * (pieces[at][1].shape[1] // 2) + first, size)
+        return ref.at[pl.ds(start, size), pl.ds(col, wide)]
+
+    def full_at(i, piece, h):
+        return part(i, pieces[chunks[i][0]][1].at[piece], h)
 
     def x_copy(i):
-        own, full = chunks[i][:2]
-        return rc(own.at[span(i, y)], full.at[k, span(i, y)], x_s.at[i], x_r.at[i], {"tp": far})
+        return rc(part(i, pieces[chunks[i][0]][0], y), full_at(i, k, y), x_s.at[i], x_r.at[i], {"tp": far})
 
     def y_copy(i):
-        at = chunks[i][1].at[far, span(i, y)]
+        at = full_at(i, far, y)
         return rc(at, at, y_s.at[i], y_r.at[i], {"grp": other_y})
 
     def dx_copy(i):
-        at = chunks[i][1].at[far, span(i, y)]
+        at = full_at(i, far, y)
         return rc(at, at, dx_s.at[i], dx_r.at[i], {"tp": mate})
 
     def dy_copy(i):
-        at = chunks[i][1].at[far, span(i, other_y)]
+        at = full_at(i, far, other_y)
         return rc(at, at, dy_s.at[i], dy_r.at[i], {"tp": mate})
 
     def own_copy(i):
-        own, full, _ = pieces[i]
+        own, full = pieces[i]
         return rc(own, full.at[k], own_s.at[i], own_r.at[i], {"tp": mate})
 
     def got(i, piece, h, send, recv):
-        at = chunks[i][1].at[piece, span(i, h)]
+        at = full_at(i, piece, h)
         rc(at, at, send.at[i], recv.at[i], {"tp": mate}).wait_recv()
 
     rows_of = lambda j: pl.ds((j % 2) * half, half)
@@ -148,8 +155,15 @@
         at = tok.at[z + 1 + j // 2, rows_of(j)]
         rc(at, at, zl_s.at[j], zl_r.at[j], {"ep": z + 1}).wait_recv()
 
-    def cf_copy(m):
-        return rc(coef, cf.at[z], cf_s.at[m - 1], cf_r.at[m - 1], {"ep": lax.rem(z + m, n_ep)})
+    def route_copies(m, here, there):
+        dev = {"ep": there}
+        return (
+            rc(route, rt.at[here], rt_s.at[m - 1], rt_r.at[m - 1], dev),
+            rc(weights, wt.at[here], wt_s.at[m - 1], wt_r.at[m - 1], dev),
+        )
+
+    def routes_out(m):
+        return route_copies(m, z, lax.rem(z + m, n_ep))
 
     tail = pl.ds(rows_mix - edge, edge)
 
@@ -162,7 +176,8 @@
     is_first, is_last = flat == 0, flat == total - 1
 
     for m in range(1, n_ep):
-        cf_copy(m).start()
+        for cp in routes_out(m):
+            cp.start()
 
     @pl.when(jnp.logical_not(is_last))
     def _():
@@ -213,14 +228,30 @@
 
         lax.fori_loop(0, rows // 32, body, 0)
 
-    norm_block(z)
-
-    def weight_step(i):
-        if i < n_chunks:
+    first_near = k - core
+    first_far = n_tp - 2 - first_near
+
+    def hidden_of(p, at):
+        g = jnp.dot(normed[at, :], full_g[p], preferred_element_type=F32)
+        u = jnp.dot(normed[at, :], full_u[p], preferred_element_type=F32)
+        hidden[p, at, :] = (jax.nn.silu(g) * u).astype(BF16)
+
+    def near_block(b):
+        norm_block(b)
+        at = pl.ds(pl.multiple_of(b * rows, rows), rows)
+
+        def body(m, _):
+            hidden_of(first_near + m, at)
+            return 0
+
+        lax.fori_loop(0, 2, body, 0)
+
+    def weight_step(i, with_y=True, with_x=True):
+        if with_x and i < n_chunks:
             got(i, far, y, x_s, x_r)
             y_copy(i).start()
             dx_copy(i).start()
-        if 1 <= i <= n_chunks:
+        if with_y and 1 <= i <= n_chunks:
             got(i - 1, far, other_y, y_s, y_r)
             dy_copy(i - 1).start()
 
@@ -233,6 +264,10 @@
         at = pieces[i][1].at[mate]
         rc(at, at, own_s.at[i], own_r.at[i], {"tp": mate}).wait_recv()
 
+    own_wait(0)
+    own_wait(1)
+    near_block(z)
+
     steps = 2 * last_z
     for s in range(steps):
         @pl.when(s < 2 * z)
@@ -250,47 +285,51 @@
         weight_step(s)
         if s % 2 == 1:
             m = s // 2 + 1
-            pl.when(z - m >= 0)(lambda: norm_block(z - m))
-            pl.when(z + m <= last_z)(lambda: norm_block(z + m))
+            pl.when(z - m >= 0)(lambda: near_block(z - m))
+            pl.when(z + m <= last_z)(lambda: near_block(z + m))
 
     mate_wait(0, 4)
-    own_wait(0)
-    own_wait(1)
-
-    def hidden_piece(p, _):
-        g = jnp.dot(normed[...], full_g[p], preferred_element_type=F32)
-        u = jnp.dot(normed[...], full_u[p], preferred_element_type=F32)
-        hidden[p] = (jax.nn.silu(g) * u).astype(BF16)
+
+    def far_piece(m, _):
+        hidden_of(first_far + m, pl.ds(0, n_ep * rows))
         return 0
 
-    lax.fori_loop(0, n_tp, hidden_piece, 0)
-    weight_step(6)
+    lax.fori_loop(0, 2, far_piece, 0)
+    weight_step(6, with_x=False)
+    weight_step(6, with_y=False)
     mate_wait(4, 6)
     own_wait(2)
     for m in range(1, n_ep):
-        at = cf.at[lax.rem(z + n_ep - m, n_ep)]
-        rc(at, at, cf_s.at[m - 1], cf_r.at[m - 1], {"ep": z}).wait_recv()
+        for cp in route_copies(m, lax.rem(z + n_ep - m, n_ep), z):
+            cp.wait_recv()
 
     eye = lax.broadcasted_iota(jnp.int32, (rows, rows), 0) == lax.broadcasted_iota(jnp.int32, (rows, rows), 1)
     columns = []
     for b in range(n_ep):
-        line = cf[b, pl.ds(z, 1), :]
+        w = wt[b]
+        share = w / jnp.sum(w, axis=0, keepdims=True)
+        line = jnp.sum(jnp.where(rt[b] == z, share, 0.0), axis=0, keepdims=True)
         columns.append(jnp.sum(jnp.where(eye, jnp.broadcast_to(line, (rows, rows)), 0.0), axis=1, keepdims=True))
     column = jnp.concatenate(columns, axis=0)
     tile = 256
 
-    def down_tile(t, _):
-        cols = pl.ds(pl.multiple_of(t * tile, tile), tile)
-        acc = jnp.dot(hidden[0], full_d[0, :, cols], preferred_element_type=F32)
-        for p in range(1, n_tp):
-            acc = acc + jnp.dot(hidden[p], full_d[p, :, cols], preferred_element_type=F32)
-        contrib[:, cols] = acc * column
-        return 0
-
-    lax.fori_loop(0, width // tile, down_tile, 0)
-
-    def own_rows(d, h):
-        return contrib[pl.ds(pl.multiple_of(d * rows + h * half, half), half), :]
+    def down_half(c):
+        def body(t, _):
+            cols = pl.ds(pl.multiple_of(c * out_cols + t * tile, tile), tile)
+            acc = jnp.dot(hidden[0], full_d[0, :, cols], preferred_element_type=F32)
+            for p in range(1, n_tp):
+                acc = acc + jnp.dot(hidden[p], full_d[p, :, cols], preferred_element_type=F32)
+            contrib[:, cols] = acc * column
+            return 0
+
+        lax.fori_loop(0, out_cols // tile, body, 0)
+
+    down_half(0)
+
+    def own_part(d, c):
+        return contrib[
+            pl.ds(pl.multiple_of(d * rows, rows), rows), pl.ds(pl.multiple_of(c * out_cols, out_cols), out_cols)
+        ]
 
     def rl_copy(s):
         return rc(out_l.at[s], in_l.at[s], rl_s.at[s], rl_r.at[s], {"ep": z - 1})
@@ -307,13 +346,16 @@
     def side(s, depth, inbox, outbox, got_fn, copy_fn, dest_fn):
         has_in = depth < last_z
 
-        @pl.when(jnp.logical_and(s >= 0, jnp.logical_and(has_in, s < 2 * (depth + 1))))
+        c, d = lax.div(s, last_z), lax.rem(s, last_z)
+        live = jnp.logical_and(s >= 0, s < steps)
+
+        @pl.when(jnp.logical_and(live, jnp.logical_and(has_in, d <= depth)))
         def _():
             got_fn(s)
 
-        @pl.when(jnp.logical_and(s >= 0, s < 2 * depth))
-        def _():
-            mine = own_rows(dest_fn(lax.div(s, 2)), lax.rem(s, 2))
+        @pl.when(jnp.logical_and(live, d < depth))
+        def _():
+            mine = own_part(dest_fn(d), c)
 
             @pl.when(has_in)
             def _():
@@ -325,42 +367,44 @@
 
             copy_fn(s).start()
 
-    for t in range(steps + 1):
+    def mixed_tile(q, _):
+        cols = pl.ds(pl.multiple_of(q * tile, tile), tile)
+        block = full_o.shape[1]
+        acc = jnp.zeros((rows_mix, tile), F32)
+        for p in range(n_tp):
+            acc = acc + jnp.dot(gated[:, p * block : (p + 1) * block], full_o[p, :, cols], preferred_element_type=F32)
+        mixed_ref[:, cols] = acc.astype(BF16)
+        return 0
+
+    for t in range(steps + last_z - 1):
+        if t == 2:
+            mate_wait(6, 7)
+            down_half(1)
         if t == steps:
-            mate_wait(6, n_chunks)
+            mate_wait(7, n_chunks)
             own_wait(3)
-
-            def mixed_tile(q, _):
-                cols = pl.ds(pl.multiple_of(q * tile, tile), tile)
-                part = full_o.shape[1]
-                acc = jnp.zeros((rows_mix, tile), F32)
-                for p in range(n_tp):
-                    acc = acc + jnp.dot(gated[:, p * part : (p + 1) * part], full_o[p, :, cols], preferred_element_type=F32)
-                mixed_ref[:, cols] = acc.astype(BF16)
-                return 0
-
             lax.fori_loop(0, width // tile, mixed_tile, 0)
         side(t - (last_z - z), z, in_l, out_l, rl_got, rl_copy, lambda b: b)
         side(t - z, last_z - z, in_r, out_r, rr_got, rr_copy, lambda b: last_z - b)
         if 7 + t <= n_chunks:
             weight_step(7 + t)
 
-    for h in range(2):
-        at = pl.ds(h * half, half)
-        mine = own_rows(z, h)
+    for c in range(2):
+        cols = pl.ds(c * out_cols, out_cols)
+        mine = own_part(z, c)
 
         @pl.when(z == 0)
         def _():
-            experts_ref[at, :] = (mine + in_l[h].astype(F32)).astype(BF16)
+            experts_ref[:, cols] = (mine + in_l[c * last_z].astype(F32)).astype(BF16)
 
         @pl.when(z == last_z)
         def _():
-            experts_ref[at, :] = (mine + in_r[h].astype(F32)).astype(BF16)
+            experts_ref[:, cols] = (mine + in_r[c * last_z].astype(F32)).astype(BF16)
 
         @pl.when(jnp.logical_and(z > 0, z < last_z))
         def _():
-            experts_ref[at, :] = (
-                mine + in_l[2 * z + h].astype(F32) + in_r[2 * (last_z - z) + h].astype(F32)
+            experts_ref[:, cols] = (
+                mine + in_l[c * last_z + z].astype(F32) + in_r[c * last_z + last_z - z].astype(F32)
             ).astype(BF16)
 
     for i in range(n_chunks):
@@ -371,7 +415,8 @@
     for i in range(len(pieces)):
         own_copy(i).wait_send()
     for m in range(1, n_ep):
-        cf_copy(m).wait_send()
+        for cp in routes_out(m):
+            cp.wait_send()
 
     @pl.when(jnp.logical_not(is_last))
     def _():
@@ -381,8 +426,8 @@
     for j in range(steps):
         pl.when(jnp.logical_and(z < last_z, j < 2 * (z + 1)))(lambda j=j: zr_send(j).wait_send())
         pl.when(jnp.logical_and(z > 0, j < 2 * (last_z - z + 1)))(lambda j=j: zl_send(j).wait_send())
-        pl.when(j < 2 * z)(lambda j=j: rl_copy(j).wait_send())
-        pl.when(j < 2 * (last_z - z))(lambda j=j: rr_copy(j).wait_send())
+        pl.when(j % last_z < z)(lambda j=j: rl_copy(j).wait_send())
+        pl.when(j % last_z < last_z - z)(lambda j=j: rr_copy(j).wait_send())
 
 
 def per_device_fused(
@@ -393,11 +438,8 @@
     rows, width = tokens_b.shape
     rows_mix, channels = conv_x.shape
     hid = w_gate.shape[2]
-    shares = route_weights / jnp.sum(route_weights, axis=-1, keepdims=True)
-    lanes = jnp.arange(-(-n_ep // 8) * 8, dtype=jnp.int32)[:, None, None]
-    coef = jnp.sum(jnp.where(route_b.T[None] == lanes, shares.T[None], 0.0), axis=1)
     edge, half, steps = 16, rows // 2, 2 * (n_ep - 1)
-    n_chunks = 10
+    n_chunks = sum(n * sum(cols) for n, cols in CUTS)
     dma = pltpu.SemaphoreType.DMA
     hbm, vmem = pl.BlockSpec(memory_space=pl.ANY), pl.BlockSpec(memory_space=pltpu.VMEM)
     return pl.pallas_call(
@@ -406,7 +448,7 @@
             jax.ShapeDtypeStruct((rows_mix, width), BF16),
             jax.ShapeDtypeStruct((rows, width), BF16),
         ),
-        in_specs=[hbm, hbm, hbm, vmem, hbm, hbm, vmem, hbm, hbm, hbm, hbm],
+        in_specs=[hbm, hbm, hbm, vmem, hbm, hbm, vmem, hbm, hbm, hbm, hbm, hbm],
         out_specs=(vmem, vmem),
         scratch_shapes=[
             pltpu.VMEM((n_tp,) + w_gate.shape[1:], BF16),
@@ -415,25 +457,26 @@
             pltpu.VMEM((n_tp,) + w_out.shape, BF16),
             pltpu.VMEM((n_ep, rows, width), BF16),
             pltpu.VMEM((n_ep * rows, width), BF16),
-            pltpu.VMEM((n_ep,) + coef.shape, F32),
+            pltpu.VMEM((n_ep, TOPK, rows), jnp.int32),
+            pltpu.VMEM((n_ep, TOPK, rows), F32),
             pltpu.VMEM((n_tp, n_ep * rows, hid), BF16),
             pltpu.VMEM((n_ep * rows, width), F32),
         ]
-        + [pltpu.VMEM((steps, half, width), BF16)] * 4
+        + [pltpu.VMEM((steps, rows, width // 2), BF16)] * 4
         + [pltpu.VMEM((rows_mix, channels), BF16)] * 3
         + [pltpu.VMEM((edge, channels), BF16)] * 2
         + [pltpu.VMEM((edge + rows_mix, 128), F32), pltpu.VMEM((rows_mix, channels), BF16)]
         + [dma((n_chunks,))] * 8
         + [dma((4,))] * 2
         + [dma((steps,))] * 4
-        + [dma((n_ep - 1,))] * 2
+        + [dma((n_ep - 1,))] * 4
         + [dma((2,))] * 2
         + [dma((steps,))] * 4
-        + [dma((9,))],
+        + [dma((10,))],
         compiler_params=pltpu.CompilerParams(
             collective_id=0, has_side_effects=True, vmem_limit_bytes=62 * 1024 * 1024
         ),
-    )(conv_x, conv_c, conv_b, conv_taps, w_out, tokens_b, norm_gain[None], coef, w_gate, w_up, w_down)
+    )(conv_x, conv_c, conv_b, conv_taps, w_out, tokens_b, norm_gain[None], route_b.T, route_weights.T, w_gate, w_up, w_down)
 
 
 def per_device(

time: 101 us -> 96.3 us (0.953); the launches traced: 101 us -> 94.4 us
  Pallas kernels: 94.1 us -> 90.5 us
  other arithmetic: 2.66 us -> 0 us
    pallas_call x1, Pallas kernels: 94.1 us -> 90.5 us  [per_device_fused(): pl.pallas_call(fused_kernel, out_shape=(jax.ShapeDtypeStruct((rows_mix, w...]
    reduce_sum x2 -> x0, other arithmetic: 1.98 us -> none  [the longest x1 1.28 us: per_device_fused(): jnp.sum(jnp.where(route_b.T[None] == lanes, shares.T[None], 0.0), axis=1)]
where the time goes in v2:
time: 96.3 us; the launch traced here: 94.4 us
  Pallas kernels  90.5 us (94%)
  local copies, waits for them, and re-layouts  3.16 us (3%)
    pallas_call x1, Pallas kernels, per_device_fused(): pl.pallas_call(fused_kernel, out_shape=(jax.ShapeDtypeStruct((rows_mix, w...  90.5 us
    unnamed x4, local copies, waits for them, and re-layouts  3.16 us

profile of v2, /device:TPU:0, one launch (start us, length us, event | category | flops | bytes accessed | tf_op | source)
XLA Modules:
  0.0 94.4 jit_solution(3197848546847867197)
XLA Ops:
  0.6 90.5 %shard_map.131 = (bf16[256,2048]{1,0:T(8,128)(2,1)}, bf16[128,2048]{1,0:T(8,128)(2,1)}) custom-call(bf16[256,2048]{1,0:T(8,128)(2,1)} %conv_x.1, bf16[256,2048]{1,0:T(8,128)(2,1)} %conv_c.1, bf16[256,2048]{1,0:T(8,128)(2,1)} %conv_b.1, f32[3,2048]{1,0:T(4,128)} %taps.1, bf16[512,2048]{1,0:T(8,128)(2,1)} %w_out.1, bf16[128,2048]{1,0:T(8,128)(2,1)} %tokens.1, ...), custom_call_target="tpu_custom_call" | custom-call | tf_op jit(solution)/shard_map/pallas_call | solution.py:445
  91.2 0.0 copy-start
  91.2 2.4 %copy.16 = bf16[256,2048]{1,0:T(8,128)(2,1)} copy(bf16[256,2048]{1,0:T(8,128)(2,1)} %get-tuple-element.4) | data formatting | bytes 2097152
  93.6 0.0 copy-done
  93.6 0.8 copy.17
Async XLA Ops:
  91.2 2.4 %copy-start = (bf16[128,2048]{1,0:T(8,128)(2,1)S(1)}, bf16[128,2048]{1,0:T(8,128)(2,1)}, u32[]{:S(2)}) copy-start(bf16[128,2048]{1,0:T(8,128)(2,1)} %get-tuple-element.5) | copy-start | bytes 1572868

commit v3 on v2

--- a/solution.py
+++ b/solution.py
@@ -445,8 +445,8 @@
     return pl.pallas_call(
         fused_kernel,
         out_shape=(
-            jax.ShapeDtypeStruct((rows_mix, width), BF16),
-            jax.ShapeDtypeStruct((rows, width), BF16),
+            pltpu.VMEM((rows_mix, width), BF16),
+            pltpu.VMEM((rows, width), BF16),
         ),
         in_specs=[hbm, hbm, hbm, vmem, hbm, hbm, vmem, hbm, hbm, hbm, hbm, hbm],
         out_specs=(vmem, vmem),
@@ -474,7 +474,7 @@
         + [dma((steps,))] * 4
         + [dma((10,))],
         compiler_params=pltpu.CompilerParams(
-            collective_id=0, has_side_effects=True, vmem_limit_bytes=62 * 1024 * 1024
+            collective_id=0, has_side_effects=True, vmem_limit_bytes=54 * 1024 * 1024
         ),
     )(conv_x, conv_c, conv_b, conv_taps, w_out, tokens_b, norm_gain[None], route_b.T, route_weights.T, w_gate, w_up, w_down)
 

time: 96.3 us -> 93.7 us (0.973)
  the two profiles are of different devices: /device:TPU:0 before, /device:TPU:26 now
where the time goes in v3:
time: 93.7 us; the launch traced here: 93.5 us
  Pallas kernels  91.1 us (97%)
  local copies, waits for them, and re-layouts  1.77 us (2%)
    pallas_call x1, Pallas kernels, per_device_fused(): pl.pallas_call(fused_kernel, out_shape=(pltpu.VMEM((rows_mix, width), BF1...  91.1 us

profile of v3, /device:TPU:26, one launch (start us, length us, event | category | flops | bytes accessed | tf_op | source)
XLA Modules:
  0.0 93.5 jit_solution(8886756415690929360)
XLA Ops:
  0.6 91.1 %shard_map.131 = (bf16[256,2048]{1,0:T(8,128)(2,1)S(1)}, bf16[128,2048]{1,0:T(8,128)(2,1)S(1)}) custom-call(bf16[256,2048]{1,0:T(8,128)(2,1)} %conv_x.1, bf16[256,2048]{1,0:T(8,128)(2,1)} %conv_c.1, bf16[256,2048]{1,0:T(8,128)(2,1)} %conv_b.1, f32[3,2048]{1,0:T(4,128)} %taps.1, bf16[512,2048]{1,0:T(8,128)(2,1)} %w_out.1, bf16[128,2048]{1,0:T(8,128)(2,1)} %tokens.1, ...), custom_call_target="tpu_custom_call" | custom-call | tf_op jit(solution)/shard_map/pallas_call | solution.py:445
  91.7 1.0 %copy.16 = bf16[256,2048]{1,0:T(8,128)(2,1)} copy(bf16[256,2048]{1,0:T(8,128)(2,1)S(1)} %get-tuple-element.2) | data formatting | bytes 2097152
  92.7 0.8 copy.17

commit v4 on v3

--- a/solution.py
+++ b/solution.py
@@ -286,6 +286,8 @@
         if s % 2 == 1:
             m = s // 2 + 1
             pl.when(z - m >= 0)(lambda: near_block(z - m))
+        m = s // 2 if s % 2 == 0 else (last_z if s == steps - 1 else 0)
+        if m:
             pl.when(z + m <= last_z)(lambda: near_block(z + m))
 
     mate_wait(0, 4)
@@ -349,16 +351,13 @@
         c, d = lax.div(s, last_z), lax.rem(s, last_z)
         live = jnp.logical_and(s >= 0, s < steps)
 
-        @pl.when(jnp.logical_and(live, jnp.logical_and(has_in, d <= depth)))
-        def _():
-            got_fn(s)
-
         @pl.when(jnp.logical_and(live, d < depth))
         def _():
             mine = own_part(dest_fn(d), c)
 
             @pl.when(has_in)
             def _():
+                got_fn(s)
                 outbox[s] = (mine + inbox[s].astype(F32)).astype(BF16)
 
             @pl.when(jnp.logical_not(has_in))
@@ -392,6 +391,9 @@
     for c in range(2):
         cols = pl.ds(c * out_cols, out_cols)
         mine = own_part(z, c)
+
+        pl.when(z < last_z)(lambda: rl_got(c * last_z + z))
+        pl.when(z > 0)(lambda: rr_got(c * last_z + last_z - z))
 
         @pl.when(z == 0)
         def _():

time: 93.7 us -> 91.8 us (0.980)
  the two profiles are of different devices: /device:TPU:26 before, /device:TPU:0 now
where the time goes in v4:
time: 91.8 us; the launch traced here: 91.6 us
  Pallas kernels  89.2 us (97%)
  local copies, waits for them, and re-layouts  1.77 us (2%)
    pallas_call x1, Pallas kernels, per_device_fused(): pl.pallas_call(fused_kernel, out_shape=(pltpu.VMEM((rows_mix, width), BF1...  89.2 us

profile of v4, /device:TPU:0, one launch (start us, length us, event | category | flops | bytes accessed | tf_op | source)
XLA Modules:
  0.0 91.6 jit_solution(14812869976151178780)
XLA Ops:
  0.6 89.2 %shard_map.131 = (bf16[256,2048]{1,0:T(8,128)(2,1)S(1)}, bf16[128,2048]{1,0:T(8,128)(2,1)S(1)}) custom-call(bf16[256,2048]{1,0:T(8,128)(2,1)} %conv_x.1, bf16[256,2048]{1,0:T(8,128)(2,1)} %conv_c.1, bf16[256,2048]{1,0:T(8,128)(2,1)} %conv_b.1, f32[3,2048]{1,0:T(4,128)} %taps.1, bf16[512,2048]{1,0:T(8,128)(2,1)} %w_out.1, bf16[128,2048]{1,0:T(8,128)(2,1)} %tokens.1, ...), custom_call_target="tpu_custom_call" | custom-call | tf_op jit(solution)/shard_map/pallas_call | solution.py:447
  89.8 1.0 %copy.16 = bf16[256,2048]{1,0:T(8,128)(2,1)} copy(bf16[256,2048]{1,0:T(8,128)(2,1)S(1)} %get-tuple-element.2) | data formatting | bytes 2097152
  90.8 0.8 copy.17
